TPU v7x, 32 devices: a whole 2x2x4 slice. The times are simulated.
32 devices in a mesh: grp: 2 (over y), sp: 4 (over z), tp: 4 (over x, core).
Axes of the slice: x: 2, y: 2, z: 4, core: 2. Of those that a mesh axis runs over, the one named last changes fastest.
Arguments:
- stream: bfloat16 [12288, 4096], P(('grp', 'sp', 'tp')), parts along dimension 0, may hold values from -6 to 6
- norm_gain: float32 [2, 4096], replicated, may hold values from 0.1 to 1.9
- mix_weight: bfloat16 [2, 4, 1024, 1024], P(None, None, 'sp', 'tp'), may hold values from -0.1875 to 0.1875
- branch_scale: float32 [2, 4096], replicated, may hold values from 0.1 to 1.9
Outputs:
- result: bfloat16 [12288, 4096], P(('grp', 'sp', 'tp')), parts along dimension 0
There are 2 independent parts, one for each index of `grp`. A program takes and returns all parts, laid end to end along the dimension named above; an argument that names none is the same for every part. Nothing has to cross between parts.
All inputs are finite; a program needn't handle non-finite values.
Results may differ from a plain program's by a relative error of at most 0.0056.
Values may be sent and summed in bfloat16 or wider, within the bound.
A program may use at most 128 MiB of HBM per device.

v0:
```python
import jax
import jax.numpy as jnp
from jax import lax
from jax.sharding import PartitionSpec as P

GW = 1024
G = 4
LAYERS = 2
epsilon = 1e-06
window_lengths = (2, 4, 8, 16)
halo_rows = 15


def from_behind(block, axis, distance):
    devices = range(lax.axis_size(axis))
    route = [(i - distance, i) for i in devices if i - distance in devices]
    return lax.ppermute(block, axis, route)


def per_device(stream, norm_gain, mix_weight, branch_scale):
    row_count = stream.shape[0]
    feature_width = stream.shape[1]
    offset = lax.axis_index(("sp", "tp")) * row_count
    counts_base = (offset + lax.iota(jnp.int32, row_count)).astype(jnp.float32) + 1.0
    residual = stream.astype(jnp.float32)
    for layer_idx in range(LAYERS):
        scale_rows = lax.rsqrt(jnp.mean(residual * residual, axis=1, keepdims=True) + epsilon)
        normed = (residual * scale_rows * norm_gain[layer_idx]).astype(jnp.bfloat16)
        earlier = from_behind(normed[row_count - halo_rows :], ("sp", "tp"), 1)
        extended = jnp.concatenate([earlier, normed], axis=0).astype(jnp.float32)
        pieces = []
        for group_idx in range(G):
            window_len = window_lengths[group_idx]
            segment = extended[:, group_idx * GW : (group_idx + 1) * GW]
            own_rows = segment[halo_rows:]
            running = own_rows
            for back_step in range(1, window_len):
                running = (
                    running + segment[halo_rows - back_step : halo_rows - back_step + row_count]
                )
            window_mean = running / jnp.minimum(counts_base, float(window_len))[:, None]
            pieces.append((window_mean - own_rows).astype(jnp.bfloat16))
        pooled = jnp.stack(pieces, axis=1)
        weight_shard = mix_weight[layer_idx]
        full_rows = lax.all_gather(weight_shard, "sp", axis=1, tiled=True)
        mixed_out = jnp.einsum(
            "rgc,gcn->rgn",
            pooled,
            lax.all_gather(full_rows, "tp", axis=2, tiled=True),
            preferred_element_type=jnp.float32,
        )
        residual = residual + mixed_out.reshape(row_count, feature_width) * branch_scale[layer_idx]
    return residual.astype(jnp.bfloat16)


def solution(mesh):
    return jax.shard_map(
        per_device,
        mesh=mesh,
        in_specs=(P(("grp", "sp", "tp"), None), P(), P(None, None, "sp", "tp"), P()),
        out_specs=P(("grp", "sp", "tp"), None),
        check_vma=False,
    )
```

profile of v0, /device:TPU:9, one launch (start us, length us, event | category | flops | bytes accessed | tf_op | source)
XLA Modules:
  0.0 248.3 jit_solution(16958773101239605890)
XLA Ops:
  6.5 2.2 fusion.69
  9.6 44.4 %all-gather.9.cloned.1.call-done = bf16[1,4,1024,256]{3,2,1,0:T(8,128)(2,1)} async-done(((bf16[1,4,256,256]{3,2,1,0:T(8,128)(2,1)}), bf16[1,4,1024,256]{3,2,1,0:T(8,128)(2,1)}) %all-gather.9.cloned.1.call-update) | async-done | bytes 2097168 | tf_op jit(solution)/shard_map/all_gather | solution.py:45
  54.8 45.3 %all-gather.13.cloned.1.call-done = bf16[1,4,1024,256]{3,2,1,0:T(8,128)(2,1)} async-done(((bf16[1,4,256,256]{3,2,1,0:T(8,128)(2,1)}), bf16[1,4,1024,256]{3,2,1,0:T(8,128)(2,1)}) %all-gather.13.cloned.1.call-update) | async-done | bytes 2097168 | tf_op jit(solution)/shard_map/all_gather | solution.py:45
  100.1 1.0 fusion.6
  101.1 1.7 copy-done.2
  102.8 4.2 %collective-permute-start = (bf16[15,4096]{1,0:T(8,128)(2,1)S(1)}, bf16[15,4096]{1,0:T(8,128)(2,1)S(1)}, u32[]{:S(2)}, u32[]{:S(2)}) collective-permute-start(bf16[15,4096]{1,0:T(8,128)(2,1)S(1)} %slice.340), channel_id=1, source_target_pairs={{0,1},{1,2},{2,3},{3,4},{4,5},{5,6},{6,7},{7,8},{8,9},{9,10},{10,1... | collective-permute-start | bytes 368648 | tf_op jit(solution)/shard_map/ppermute | solution.py:17
  107.1 1.8 collective-permute-done
  108.9 3.2 %maximum_convert_fusion = f32[399,4096]{1,0:T(8,128)S(1)} fusion(bf16[384,4096]{1,0:T(8,128)(2,1)} %copy-done.2, bf16[15,4096]{1,0:T(8,128)(2,1)S(1)} %collective-permute-done), kind=kLoop, calls=%fused_computation.13 | loop fusion | flops 6537216 | bytes 9805824 | tf_op jit(solution)/shard_map/convert_element_type | solution.py:30
  112.2 3.3 %fusion.62 = bf16[384,1,1024]{2,0,1:T(8,128)(2,1)} fusion(f32[384]{0:T(512)S(1)} %fusion.63, f32[399,4096]{1,0:T(8,128)S(1)} %maximum_convert_fusion), kind=kLoop, calls=%fused_computation.114 | loop fusion | flops 7077888 | bytes 25953792 | tf_op jit(solution)/shard_map/stack | solution.py:43
  115.4 3.6 %fusion.56 = (bf16[384,1,1024]{2,0,1:T(8,128)(2,1)}, bf16[384,1,1024]{2,0,1:T(8,128)(2,1)}, bf16[384,1,1024]{2,0,1:T(8,128)(2,1)}) fusion(f32[384]{0:T(512)S(1)} %fusion.66, f32[399,4096]{1,0:T(8,128)S(1)} %maximum_convert_fusion, f32[384]{0:T(512)S(1)} %get-tuple-element.18, f32[384]{0:T(512)S(1)} %get-tuple-element.17), kind=kLoop, calls=%fused_computation.108 | loop fusion | flops 7864320 | bytes 24384000 | tf_op jit(solution)/shard_map/stack | solution.py:43
  119.0 43.0 %all-gather.11.cloned.1.call-done = bf16[1,4,1024,1024]{3,2,1,0:T(8,128)(2,1)} async-done(((bf16[1,4,1024,256]{3,2,1,0:T(8,128)(2,1)}), bf16[1,4,1024,1024]{3,2,1,0:T(8,128)(2,1)}) %all-gather.11.cloned.1.call-update) | async-done | bytes 8388624 | tf_op jit(solution)/shard_map/all_gather | solution.py:49
  162.0 7.8 %fusion.21 = f32[4,48,8,1024]{3,2,1,0:T(8,128)S(1)} fusion(bf16[1,4,1024,1024]{3,2,1,0:T(8,128)(2,1)} %all-gather.11.cloned.1.call-done, bf16[384,1,1024]{2,0,1:T(8,128)(2,1)} %fusion.62, bf16[384,1,1024]{2,0,1:T(8,128)(2,1)} %get-tuple-element.10, bf16[384,1,1024]{2,0,1:T(8,128)(2,1)} %get-tuple-element.9, bf16[384,1,1024]{2,0,1:T(8,128)(2,1)} %get-tuple-element.8), kind=kOutput, calls=%fused_computation.29 | convolution fusion | flops 3225944064 | bytes 17825792 | tf_op jit(solution)/shard_map/rgc,gcn->rgn/dot_general | solution.py:46
  170.4 1.2 multiply_reduce_fusion
  171.6 2.0 copy-done
  173.7 1.6 multiply_convert_fusion
  175.3 2.3 collective-permute-start.1
  177.6 4.6 %collective-permute-done.1 = bf16[15,4096]{1,0:T(8,128)(2,1)S(1)} collective-permute-done((bf16[15,4096]{1,0:T(8,128)(2,1)S(1)}, bf16[15,4096]{1,0:T(8,128)(2,1)S(1)}, u32[]{:S(2)}, u32[]{:S(2)}) %collective-permute-start.1) | collective-permute-done | bytes 122912 | tf_op jit(solution)/shard_map/ppermute | solution.py:17
  182.2 0.9 maximum_convert_fusion.1
  183.1 3.3 %fusion.61 = bf16[384,1,1024]{2,0,1:T(8,128)(2,1)} fusion(f32[384]{0:T(512)S(1)} %fusion.63, f32[399,4096]{1,0:T(8,128)S(1)} %maximum_convert_fusion.1), kind=kLoop, calls=%fused_computation.113 | loop fusion | flops 7077888 | bytes 25953792 | tf_op jit(solution)/shard_map/stack | solution.py:43
  186.4 3.5 %fusion.55 = (bf16[384,1,1024]{2,0,1:T(8,128)(2,1)}, bf16[384,1,1024]{2,0,1:T(8,128)(2,1)}, bf16[384,1,1024]{2,0,1:T(8,128)(2,1)}) fusion(f32[384]{0:T(512)S(1)} %fusion.66, f32[399,4096]{1,0:T(8,128)S(1)} %maximum_convert_fusion.1, f32[384]{0:T(512)S(1)} %get-tuple-element.18, f32[384]{0:T(512)S(1)} %get-tuple-element.17), kind=kLoop, calls=%fused_computation.107 | loop fusion | flops 7864320 | bytes 24384000 | tf_op jit(solution)/shard_map/stack | solution.py:43
  189.9 34.3 %all-gather.15.cloned.1.call-done = bf16[1,4,1024,1024]{3,2,1,0:T(8,128)(2,1)} async-done(((bf16[1,4,1024,256]{3,2,1,0:T(8,128)(2,1)}), bf16[1,4,1024,1024]{3,2,1,0:T(8,128)(2,1)}) %all-gather.15.cloned.1.call-update) | async-done | bytes 8388624 | tf_op jit(solution)/shard_map/all_gather | solution.py:49
  224.3 7.9 %fusion.26 = f32[4,48,8,1024]{3,2,1,0:T(8,128)S(1)} fusion(bf16[1,4,1024,1024]{3,2,1,0:T(8,128)(2,1)} %all-gather.15.cloned.1.call-done, bf16[384,1,1024]{2,0,1:T(8,128)(2,1)} %fusion.61, bf16[384,1,1024]{2,0,1:T(8,128)(2,1)} %get-tuple-element.7, bf16[384,1,1024]{2,0,1:T(8,128)(2,1)} %get-tuple-element.6, bf16[384,1,1024]{2,0,1:T(8,128)(2,1)} %get-tuple-element.5), kind=kOutput, calls=%fused_computation.30 | convolution fusion | flops 3225944064 | bytes 17825792 | tf_op jit(solution)/shard_map/rgc,gcn->rgn/dot_general | solution.py:46
  232.2 3.4 %copy.8 = f32[4,48,8,1024]{3,2,0,1:T(8,128)} copy(f32[4,48,8,1024]{3,2,1,0:T(8,128)S(1)} %fusion.26) | data formatting | bytes 12582912 | tf_op jit(solution)/shard_map/reshape | solution.py:52
  235.6 6.2 %add_convert_fusion = bf16[384,4096]{1,0:T(8,128)(2,1)} fusion(f32[384,4096]{1,0:T(8,128)} %bitcast.43, f32[4096]{0:T(1024)S(1)} %bitcast.47, f32[384,4096]{1,0:T(8,128)S(1)} %bitcast.42, f32[4096]{0:T(1024)S(1)} %bitcast.46, bf16[384,4096]{1,0:T(8,128)(2,1)S(1)} %copy-done.1), kind=kLoop, calls=%fused_computation.10 | loop fusion | flops 9437184 | bytes 18907136 | tf_op jit(solution)/shard_map/convert_element_type | solution.py:53
  (32 shorter events, 2.3 us)
Async XLA Ops:
  6.5 47.4 %all-gather.9.cloned.1.call-start = ((), (), s32[]{:S(2)}) async-start(), calls=%async_computation | async-start | bytes 2621440 | tf_op jit(solution)/shard_map/all_gather | solution.py:45
  8.8 45.3 %copy-start.1 = (bf16[384,4096]{1,0:T(8,128)(2,1)S(1)}, bf16[384,4096]{1,0:T(8,128)(2,1)}, u32[]{:S(2)}) copy-start(bf16[384,4096]{1,0:T(8,128)(2,1)} %param.4) | copy-start | bytes 9437188
  8.8 91.2 %all-gather.13.cloned.1.call-start = ((), (), s32[]{:S(2)}) async-start(), calls=%async_computation.2 | async-start | bytes 2621440 | tf_op jit(solution)/shard_map/all_gather | solution.py:45
  9.6 152.5 %all-gather.11.cloned.1.call-start = ((), (), s32[]{:S(2)}) async-start(), calls=%async_computation.1 | async-start | bytes 10485760 | tf_op jit(solution)/shard_map/all_gather | solution.py:49
  54.0 170.3 %all-gather.15.cloned.1.call-start = ((), (), s32[]{:S(2)}) async-start(), calls=%async_computation.3 | async-start | bytes 10485760 | tf_op jit(solution)/shard_map/all_gather | solution.py:49
  54.7 45.3 %copy-start.3 = (f32[2,4096]{1,0:T(2,128)S(1)}, f32[2,4096]{1,0:T(2,128)}, u32[]{:S(2)}) copy-start(f32[2,4096]{1,0:T(2,128)} %param.5) | copy-start | bytes 98308
  100.1 6.9 %copy-start.4 = (f32[2,4096]{1,0:T(2,128)S(1)}, f32[2,4096]{1,0:T(2,128)}, u32[]{:S(2)}) copy-start(f32[2,4096]{1,0:T(2,128)} %param.7) | copy-start | bytes 98308
  101.1 1.7 copy-start.2
  102.8 6.1 %collective-permute-start = (bf16[15,4096]{1,0:T(8,128)(2,1)S(1)}, bf16[15,4096]{1,0:T(8,128)(2,1)S(1)}, u32[]{:S(2)}, u32[]{:S(2)}) collective-permute-start(bf16[15,4096]{1,0:T(8,128)(2,1)S(1)} %slice.340), channel_id=1, source_target_pairs={{0,1},{1,2},{2,3},{3,4},{4,5},{5,6},{6,7},{7,8},{8,9},{9,10},{10,1... | collective-permute-start | bytes 368648 | tf_op jit(solution)/shard_map/ppermute | solution.py:17
  170.4 3.3 %copy-start = (f32[4,48,8,1024]{3,2,0,1:T(8,128)}, f32[4,48,8,1024]{3,2,0,1:T(8,128)S(1)}, u32[]{:S(2)}) copy-start(f32[4,48,8,1024]{3,2,0,1:T(8,128)S(1)} %copy.7) | copy-start | bytes 18874372
  175.3 6.9 %collective-permute-start.1 = (bf16[15,4096]{1,0:T(8,128)(2,1)S(1)}, bf16[15,4096]{1,0:T(8,128)(2,1)S(1)}, u32[]{:S(2)}, u32[]{:S(2)}) collective-permute-start(bf16[15,4096]{1,0:T(8,128)(2,1)S(1)} %slice.371), channel_id=1, source_target_pairs={{0,1},{1,2},{2,3},{3,4},{4,5},{5,6},{6,7},{7,8},{8,9},{9,10},{10,1... | collective-permute-start | bytes 368648 | tf_op jit(solution)/shard_map/ppermute | solution.py:17
  224.3 11.3 %slice-start = ((s8[6291456]{0:T(1024)(128)(4,1)}), s8[4194304]{0:T(1024)(128)(4,1)S(1)}, s32[]{:S(2)}) async-start(s8[6291456]{0:T(1024)(128)(4,1)} %bitcast.40), calls=%async_computation.4 | async-start | bytes 8388608
  224.3 11.3 %slice-start.1 = ((s8[6291456]{0:T(1024)(128)(4,1)}), s8[2097152]{0:T(1024)(128)(4,1)S(1)}, s32[]{:S(2)}) async-start(s8[6291456]{0:T(1024)(128)(4,1)} %bitcast.40), calls=%async_computation.5 | async-start | bytes 4194304
Sparse Core Ops, SparseCore 0:
  8.9 44.9 all-gather.8
  55.5 44.4 all-gather.12
  101.6 60.4 all-gather.10
  163.4 60.7 all-gather.14
where the time goes:
time: 249 us; the launch traced here: 248 us
  waiting for transfers between devices  174 us (70%)
  other arithmetic  28.5 us (11%)
  matrix products  15.6 us (6%)
  between operations  13.3 us (5%)
  local copies, waits for them, and re-layouts  10.1 us (4%)
  starting transfers between devices  6.56 us (3%)
    all_gather x2, waiting for transfers between devices, per_device(): full_rows = lax.all_gather(weight_shard, 'sp', axis=1, tiled=True)  89.6 us
    all_gather x2, waiting for transfers between devices, per_device(): lax.all_gather(full_rows, 'tp', axis=2, tiled=True)  77.3 us
    dot_general x2, matrix products, per_device(): jnp.einsum('rgc,gcn->rgn', pooled, lax.all_gather(full_rows, 'tp', axis=2...  15.6 us
    another operation x4, other arithmetic, per_device(): pooled = jnp.stack(pieces, axis=1)  13.6 us
    ppermute x2, waiting for transfers between devices, from_behind(): return lax.ppermute(block, axis, route)  6.48 us
    ppermute x2, starting transfers between devices, from_behind(): return lax.ppermute(block, axis, route)  6.44 us
    convert_element_type x1, other arithmetic, per_device(): return residual.astype(jnp.bfloat16)  6.2 us
  transfers between devices with their start and end apart: 6, of which 6 were waited for; matrix products, arithmetic and copies ran while one was open for 12% of the time, Pallas kernels for 0%

commit v1 on v0

--- a/solution.py
+++ b/solution.py
@@ -9,6 +9,33 @@
 epsilon = 1e-06
 window_lengths = (2, 4, 8, 16)
 halo_rows = 15
+
+
+def laid_out(pieces, dim):
+    dims = list(pieces.shape[1:])
+    dims[dim] *= pieces.shape[0]
+    return jnp.moveaxis(pieces, 0, dim).reshape(dims)
+
+
+def ring_apply(array, axis, dim, apply, out_dim):
+    devices, position, width = (lax.axis_size(axis), lax.axis_index(axis), array.shape[dim])
+    right = [(i, (i + 1) % devices) for i in range(devices)]
+    behind = [(i, (i - 1) % devices) for i in range(devices)]
+    halfway = devices // 2
+    parts = {}
+    from_left = from_right = array
+    for step in range(halfway + 1):
+        next_left = lax.ppermute(from_left, axis, right) if step < halfway else None
+        next_right = (
+            lax.ppermute(from_right, axis, behind) if step < devices - halfway - 1 else None
+        )
+        parts[-step] = apply(from_left, (position - step) % devices * width)
+        if 0 < step < devices - halfway:
+            parts[step] = apply(from_right, (position + step) % devices * width)
+        from_left, from_right = (next_left, next_right)
+    parts = jnp.stack([parts[k] for k in sorted(parts)])
+    parts = parts[(jnp.arange(devices) - position + halfway) % devices]
+    return laid_out(parts, out_dim)
 
 
 def from_behind(block, axis, distance):
@@ -43,11 +70,14 @@
         pooled = jnp.stack(pieces, axis=1)
         weight_shard = mix_weight[layer_idx]
         full_rows = lax.all_gather(weight_shard, "sp", axis=1, tiled=True)
-        mixed_out = jnp.einsum(
-            "rgc,gcn->rgn",
-            pooled,
-            lax.all_gather(full_rows, "tp", axis=2, tiled=True),
-            preferred_element_type=jnp.float32,
+        mixed_out = ring_apply(
+            full_rows,
+            "tp",
+            2,
+            lambda part, at: jnp.einsum(
+                "rgc,gcn->rgn", pooled, part, preferred_element_type=jnp.float32
+            ),
+            2,
         )
         residual = residual + mixed_out.reshape(row_count, feature_width) * branch_scale[layer_idx]
     return residual.astype(jnp.bfloat16)

time: 249 us -> 262 us (1.052); the launches traced: 248 us -> 258 us
  waiting for transfers between devices: 174 us -> 113 us
  local copies, waits for them, and re-layouts: 10.1 us -> 52.8 us
  starting transfers between devices: 6.56 us -> 17.3 us
  other arithmetic: 28.5 us -> 39.2 us
  matrix products: 15.6 us -> 22.1 us
    all_gather x2 -> x0, waiting for transfers between devices: 77.3 us -> none  [per_device(): lax.all_gather(full_rows, 'tp', axis=2, tiled=True)]
    ppermute x0 -> x6, waiting for transfers between devices: none -> 77 us  [the longest x4 77 us: ring_apply(): next_left = lax.ppermute(from_left, axis, right) if step < halfway else None]
    all_gather x2, waiting for transfers between devices: 89.6 us -> 35.8 us  [per_device(): full_rows = lax.all_gather(weight_shard, 'sp', axis=1, tiled=True)]
    transpose x0 -> x2, local copies, waits for them, and re-layouts: none -> 18.9 us  [laid_out(): return jnp.moveaxis(pieces, 0, dim).reshape(dims)]
    another operation x0 -> x2, local copies, waits for them, and re-layouts: none -> 16.5 us  [per_device(): mixed_out.reshape(row_count, feature_width) * branch_scale[layer_idx]]
    gather x0 -> x2, local copies, waits for them, and re-layouts: none -> 12.7 us  [ring_apply(): parts = parts[(jnp.arange(devices) - position + halfway) % devices]]
    ppermute x0 -> x6, starting transfers between devices: none -> 9.18 us  [the longest x4 9.12 us: ring_apply(): next_left = lax.ppermute(from_left, axis, right) if step < halfway else None]
    dot_general x2 -> x8, matrix products: 15.6 us -> 22.1 us  [per_device(): jnp.einsum('rgc,gcn->rgn', pooled, part, preferred_element_type=jnp.float32)]
  transfers between devices with their start and end apart: 6 -> 10, of which waited for: 6 -> 5; matrix products, arithmetic and copies ran while one was open for 12% -> 28% of each run, Pallas kernels for 0% -> 0%
where the time goes in v1:
time: 262 us; the launch traced here: 258 us
  waiting for transfers between devices  113 us (43%)
  local copies, waits for them, and re-layouts  52.8 us (20%)
  other arithmetic  39.2 us (15%)
  matrix products  22.1 us (8%)
  starting transfers between devices  17.3 us (7%)
  between operations  13.7 us (5%)
    ppermute x4, waiting for transfers between devices, ring_apply(): next_left = lax.ppermute(from_left, axis, right) if step < halfway else None  77 us
    all_gather x2, waiting for transfers between devices, per_device(): full_rows = lax.all_gather(weight_shard, 'sp', axis=1, tiled=True)  35.8 us
    dot_general x8, matrix products, per_device(): jnp.einsum('rgc,gcn->rgn', pooled, part, preferred_element_type=jnp.float32)  22.1 us
    transpose x2, local copies, waits for them, and re-layouts, laid_out(): return jnp.moveaxis(pieces, 0, dim).reshape(dims)  18.9 us
    another operation x2, local copies, waits for them, and re-layouts, per_device(): mixed_out.reshape(row_count, feature_width) * branch_scale[layer_idx]  16.5 us
    gather x2, local copies, waits for them, and re-layouts, ring_apply(): parts = parts[(jnp.arange(devices) - position + halfway) % devices]  12.7 us
    another operation x4, other arithmetic, per_device(): pooled = jnp.stack(pieces, axis=1)  12.4 us
    ppermute x4, starting transfers between devices, ring_apply(): next_left = lax.ppermute(from_left, axis, right) if step < halfway else None  9.12 us
  transfers between devices with their start and end apart: 10, of which 5 were waited for; matrix products, arithmetic and copies ran while one was open for 28% of the time, Pallas kernels for 0%

profile of v1, /device:TPU:9, one launch (start us, length us, event | category | flops | bytes accessed | tf_op | source)
XLA Modules:
  0.0 258.0 jit_solution(574488837918457934)
XLA Ops:
  14.4 3.7 %collective-permute-start = (bf16[15,4096]{1,0:T(8,128)(2,1)S(1)}, bf16[15,4096]{1,0:T(8,128)(2,1)S(1)}, u32[]{:S(2)}, u32[]{:S(2)}) collective-permute-start(bf16[15,4096]{1,0:T(8,128)(2,1)S(1)} %slice.344), channel_id=1, source_target_pairs={{0,1},{1,2},{2,3},{3,4},{4,5},{5,6},{6,7},{7,8},{8,9},{9,10},{10,1... | collective-permute-start | bytes 368648 | tf_op jit(solution)/shard_map/ppermute | solution.py:44
  18.2 35.8 %all-gather.5.cloned.1.call-done = bf16[1,4,1024,256]{3,2,1,0:T(8,128)(2,1)} async-done(((bf16[1,4,256,256]{3,2,1,0:T(8,128)(2,1)}), bf16[1,4,1024,256]{3,2,1,0:T(8,128)(2,1)}) %all-gather.5.cloned.1.call-update) | async-done | bytes 2097168 | tf_op jit(solution)/shard_map/all_gather | solution.py:72
  54.0 3.0 %collective-permute-start.1 = (bf16[4,1024,256]{2,1,0:T(8,128)(2,1)}, bf16[4,1024,256]{2,1,0:T(8,128)(2,1)}, u32[]{:S(2)}, u32[]{:S(2)}) collective-permute-start(bf16[4,1024,256]{2,1,0:T(8,128)(2,1)} %bitcast.5), channel_id=1, source_target_pairs={{0,1},{1,2},{2,3},{3,0},{4,5},{5,6},{6,7},{7,4},{8,9},{9,10},{10,1... | collective-permute-start | bytes 6291464 | tf_op jit(solution)/shard_map/ppermute | solution.py:28
  59.8 3.6 %fusion.28 = (bf16[384,1,1024]{2,0,1:T(8,128)(2,1)}, bf16[384,1,1024]{2,0,1:T(8,128)(2,1)}, bf16[384,1,1024]{2,0,1:T(8,128)(2,1)}) fusion(f32[384]{0:T(512)S(1)} %fusion.38, f32[399,4096]{1,0:T(8,128)S(1)} %maximum_convert_fusion, f32[384]{0:T(512)S(1)} %get-tuple-element.18, f32[384]{0:T(512)S(1)} %get-tuple-element.17), kind=kLoop, calls=%fused_computation.102 | loop fusion | flops 7864320 | bytes 24384000 | tf_op jit(solution)/shard_map/stack | solution.py:70
  63.4 32.8 %collective-permute-done.1 = bf16[4,1024,256]{2,1,0:T(8,128)(2,1)} collective-permute-done((bf16[4,1024,256]{2,1,0:T(8,128)(2,1)}, bf16[4,1024,256]{2,1,0:T(8,128)(2,1)}, u32[]{:S(2)}, u32[]{:S(2)}) %collective-permute-start.1) | collective-permute-done | bytes 2097184 | tf_op jit(solution)/shard_map/ppermute | solution.py:28
  98.6 3.3 %fusion.34 = bf16[384,1,1024]{2,0,1:T(8,128)(2,1)} fusion(f32[384]{0:T(512)S(1)} %fusion.35, f32[399,4096]{1,0:T(8,128)S(1)} %maximum_convert_fusion), kind=kLoop, calls=%fused_computation.108 | loop fusion | flops 7077888 | bytes 25953792 | tf_op jit(solution)/shard_map/stack | solution.py:70
  103.8 3.6 %convolution_bitcast_fusion.5 = f32[1,384,4,256]{3,1,2,0:T(8,128)S(1)} fusion(bf16[1,4,1024,256]{3,2,1,0:T(8,128)(2,1)} %all-gather.5.cloned.1.call-done, bf16[384,1,1024]{2,0,1:T(8,128)(2,1)} %fusion.34, bf16[384,1,1024]{2,0,1:T(8,128)(2,1)} %get-tuple-element.10, bf16[384,1,1024]{2,0,1:T(8,128)(2,1)} %get-tuple-element.9, ...), kind=kOutput, calls=%fused_computation.98 | convolution fusion | flops 810024960 | bytes 6815744 | tf_op jit(solution)/shard_map/rgc,gcn->rgn/dot_general | solution.py:77
  107.5 3.4 %convolution_bitcast_fusion.6 = f32[1,384,4,256]{3,1,2,0:T(8,128)S(1)} fusion(bf16[4,1024,256]{2,1,0:T(8,128)(2,1)} %collective-permute-done.1, bf16[384,1,1024]{2,0,1:T(8,128)(2,1)S(1)} %copy-done.3, bf16[384,1,1024]{2,0,1:T(8,128)(2,1)S(1)} %copy-done.6, bf16[384,1,1024]{2,0,1:T(8,128)(2,1)S(1)} %copy-done.5, bf16[384,1,1024]{2,0,1:T(8,128)(2,1)S(1)} %copy-done.4), kind=kOutput, calls=%fused_computation.99 | convolution fusion | flops 810024960 | bytes 6815744 | tf_op jit(solution)/shard_map/rgc,gcn->rgn/dot_general | solution.py:77
  111.0 3.4 %convolution_bitcast_fusion.4 = f32[1,384,4,256]{3,1,2,0:T(8,128)S(1)} fusion(bf16[4,1024,256]{2,1,0:T(8,128)(2,1)} %collective-permute-done.3, bf16[384,1,1024]{2,0,1:T(8,128)(2,1)S(1)} %copy-done.3, bf16[384,1,1024]{2,0,1:T(8,128)(2,1)S(1)} %copy-done.6, bf16[384,1,1024]{2,0,1:T(8,128)(2,1)S(1)} %copy-done.5, bf16[384,1,1024]{2,0,1:T(8,128)(2,1)S(1)} %copy-done.4), kind=kOutput, calls=%fused_computation.97 | convolution fusion | flops 810024960 | bytes 6815744 | tf_op jit(solution)/shard_map/rgc,gcn->rgn/dot_general | solution.py:77
  114.4 10.8 %collective-permute-done.2 = bf16[4,1024,256]{2,1,0:T(8,128)(2,1)} collective-permute-done((bf16[4,1024,256]{2,1,0:T(8,128)(2,1)}, bf16[4,1024,256]{2,1,0:T(8,128)(2,1)}, u32[]{:S(2)}, u32[]{:S(2)}) %collective-permute-start.2) | collective-permute-done | bytes 2097184 | tf_op jit(solution)/shard_map/ppermute | solution.py:28
  125.2 3.4 %convolution_bitcast_fusion.7 = f32[1,384,4,256]{3,1,2,0:T(8,128)S(1)} fusion(bf16[4,1024,256]{2,1,0:T(8,128)(2,1)} %collective-permute-done.2, bf16[384,1,1024]{2,0,1:T(8,128)(2,1)S(1)} %copy-done.3, bf16[384,1,1024]{2,0,1:T(8,128)(2,1)S(1)} %copy-done.6, bf16[384,1,1024]{2,0,1:T(8,128)(2,1)S(1)} %copy-done.5, bf16[384,1,1024]{2,0,1:T(8,128)(2,1)S(1)} %copy-done.4), kind=kOutput, calls=%fused_computation.100 | convolution fusion | flops 810024960 | bytes 6815744 | tf_op jit(solution)/shard_map/rgc,gcn->rgn/dot_general | solution.py:77
  131.5 6.4 %gather_fusion = f32[4,384,4,256]{3,1,2,0:T(8,128)} fusion(f32[4,384,4,256]{3,1,2,0:T(8,128)} %pad_maximum_fusion, s32[1024]{0:T(1024)S(1)} %pad_clamp_fusion), kind=kCustom, calls=%fused_computation | custom fusion | bytes 12582928 | tf_op jit(solution)/shard_map/gather | solution.py:37
  137.9 9.4 %copy.5 = f32[384,4,4,256]{3,2,1,0:T(4,128)} copy(f32[384,4,4,256]{3,0,1,2:T(8,128)} %bitcast.69) | data formatting | bytes 12582912 | tf_op jit(solution)/shard_map/transpose | solution.py:17
  147.3 8.3 %reshape_reshape.6 = f32[384,4096]{1,0:T(8,128)} reshape(f32[384,4,4,256]{3,2,1,0:T(4,128)} %copy.5) | data formatting | bytes 12582912 | tf_op jit(solution)/shard_map/reshape;reshape | solution.py:82
  155.6 4.0 %multiply_reduce_fusion = f32[384]{0:T(512)S(1)} fusion(f32[384,4096]{1,0:T(8,128)} %reshape_reshape.6, f32[4096]{0:T(1024)S(1)} %bitcast.70, bf16[384,4096]{1,0:T(8,128)(2,1)S(1)} %copy-done.1), kind=kLoop, calls=%fused_computation.12 | loop fusion | flops 7863936 | bytes 9455104 | tf_op jit(solution)/shard_map/reduce_sum | solution.py:54
  161.8 4.4 %collective-permute-start.4 = (bf16[15,4096]{1,0:T(8,128)(2,1)S(1)}, bf16[15,4096]{1,0:T(8,128)(2,1)S(1)}, u32[]{:S(2)}, u32[]{:S(2)}) collective-permute-start(bf16[15,4096]{1,0:T(8,128)(2,1)S(1)} %slice.375), channel_id=1, source_target_pairs={{0,1},{1,2},{2,3},{3,4},{4,5},{5,6},{6,7},{7,8},{8,9},{9,10},{10,1... | collective-permute-start | bytes 368648 | tf_op jit(solution)/shard_map/ppermute | solution.py:44
  169.0 3.0 %fusion.27 = (bf16[384,1,1024]{2,0,1:T(8,128)(2,1)S(1)}, bf16[384,1,1024]{2,0,1:T(8,128)(2,1)S(1)}, bf16[384,1,1024]{2,0,1:T(8,128)(2,1)S(1)}) fusion(f32[384]{0:T(512)S(1)} %fusion.38, f32[399,4096]{1,0:T(8,128)S(1)} %maximum_convert_fusion.1, f32[384]{0:T(512)S(1)} %get-tuple-element.18, f32[384]{0:T(512)S(1)} %get-tuple-element.17), kind=kLoop, calls=%fused_computation.101 | loop fusion | flops 7864320 | bytes 24384000 | tf_op jit(solution)/shard_map/stack | solution.py:70
  174.5 3.4 %convolution_bitcast_fusion.2 = f32[1,384,4,256]{3,1,2,0:T(8,128)S(1)} fusion(bf16[4,1024,256]{2,1,0:T(8,128)(2,1)} %collective-permute-done.5, bf16[384,1,1024]{2,0,1:T(8,128)(2,1)S(1)} %fusion.33, bf16[384,1,1024]{2,0,1:T(8,128)(2,1)S(1)} %get-tuple-element.7, bf16[384,1,1024]{2,0,1:T(8,128)(2,1)S(1)} %get-tuple-element.6, ...), kind=kOutput, calls=%fused_computation.95 | convolution fusion | flops 810024960 | bytes 6815744 | tf_op jit(solution)/shard_map/rgc,gcn->rgn/dot_general | solution.py:77
  179.6 33.5 %collective-permute-done.6 = bf16[4,1024,256]{2,1,0:T(8,128)(2,1)S(1)} collective-permute-done((bf16[4,1024,256]{2,1,0:T(8,128)(2,1)}, bf16[4,1024,256]{2,1,0:T(8,128)(2,1)S(1)}, u32[]{:S(2)}, u32[]{:S(2)}) %collective-permute-start.6) | collective-permute-done | bytes 2097184 | tf_op jit(solution)/shard_map/ppermute | solution.py:28
  216.2 2.8 %pad_maximum_fusion.1 = f32[4,384,4,256]{3,1,2,0:T(8,128)} fusion(f32[1,384,4,256]{3,1,2,0:T(8,128)S(1)} %convolution_bitcast_fusion, f32[1,384,4,256]{3,1,2,0:T(8,128)S(1)} %convolution_bitcast_fusion.1, f32[1,384,4,256]{3,1,2,0:T(8,128)S(1)} %convolution_bitcast_fusion.2, f32[1,384,4,256]{3,1,2,0:T(8,128)S(1)} %convolution_bitcast_fusion.3), kind=kLoop, calls=%fused_computation.9 | loop fusion | flops 4718592 | bytes 12582912 | tf_op jit(solution)/shard_map/stack | solution.py:36
  219.1 6.3 %gather_fusion.1 = f32[4,384,4,256]{3,1,2,0:T(8,128)} fusion(f32[4,384,4,256]{3,1,2,0:T(8,128)} %pad_maximum_fusion.1, s32[1024]{0:T(1024)S(1)} %pad_clamp_fusion), kind=kCustom, calls=%fused_computation.1 | custom fusion | bytes 12582928 | tf_op jit(solution)/shard_map/gather | solution.py:37
  225.4 9.4 %copy.6 = f32[384,4,4,256]{3,2,1,0:T(4,128)} copy(f32[384,4,4,256]{3,0,1,2:T(8,128)} %bitcast.68) | data formatting | bytes 12582912 | tf_op jit(solution)/shard_map/transpose | solution.py:17
  234.9 8.3 %reshape_reshape.7 = f32[384,4096]{1,0:T(8,128)} reshape(f32[384,4,4,256]{3,2,1,0:T(4,128)} %copy.6) | data formatting | bytes 12582912 | tf_op jit(solution)/shard_map/reshape;reshape | solution.py:82
  243.1 8.0 %add_convert_fusion = bf16[384,4096]{1,0:T(8,128)(2,1)} fusion(f32[384,4096]{1,0:T(8,128)} %reshape_reshape.7, f32[4096]{0:T(1024)S(1)} %bitcast.73, f32[384,4096]{1,0:T(8,128)} %reshape_reshape.6, f32[4096]{0:T(1024)S(1)} %bitcast.72, bf16[384,4096]{1,0:T(8,128)(2,1)S(1)} %copy-done.1), kind=kLoop, calls=%fused_computation.10 | loop fusion | flops 9437184 | bytes 18907136 | tf_op jit(solution)/shard_map/convert_element_type | solution.py:83
  (57 shorter events, 30.2 us)
Async XLA Ops:
  6.5 47.4 %all-gather.5.cloned.1.call-start = ((), (), s32[]{:S(2)}) async-start(), calls=%async_computation | async-start | bytes 2621440 | tf_op jit(solution)/shard_map/all_gather | solution.py:72
  8.8 2.8 %copy-start.7 = (f32[2,4096]{1,0:T(2,128)S(1)}, f32[2,4096]{1,0:T(2,128)}, u32[]{:S(2)}) copy-start(f32[2,4096]{1,0:T(2,128)} %param.5) | copy-start | bytes 98308
  8.8 2.9 %copy-start.1 = (bf16[384,4096]{1,0:T(8,128)(2,1)S(1)}, bf16[384,4096]{1,0:T(8,128)(2,1)}, u32[]{:S(2)}) copy-start(bf16[384,4096]{1,0:T(8,128)(2,1)} %param.4) | copy-start | bytes 9437188
  8.8 93.1 %all-gather.7.cloned.1.call-start = ((), (), s32[]{:S(2)}) async-start(), calls=%async_computation.1 | async-start | bytes 2621440 | tf_op jit(solution)/shard_map/all_gather | solution.py:72
  11.7 6.5 %copy-start.8 = (f32[2,4096]{1,0:T(2,128)S(1)}, f32[2,4096]{1,0:T(2,128)}, u32[]{:S(2)}) copy-start(f32[2,4096]{1,0:T(2,128)} %param.7) | copy-start | bytes 98308
  12.7 1.7 copy-start.2
  14.4 42.6 %collective-permute-start = (bf16[15,4096]{1,0:T(8,128)(2,1)S(1)}, bf16[15,4096]{1,0:T(8,128)(2,1)S(1)}, u32[]{:S(2)}, u32[]{:S(2)}) collective-permute-start(bf16[15,4096]{1,0:T(8,128)(2,1)S(1)} %slice.344), channel_id=1, source_target_pairs={{0,1},{1,2},{2,3},{3,4},{4,5},{5,6},{6,7},{7,8},{8,9},{9,10},{10,1... | collective-permute-start | bytes 368648 | tf_op jit(solution)/shard_map/ppermute | solution.py:44
  54.0 42.2 %collective-permute-start.1 = (bf16[4,1024,256]{2,1,0:T(8,128)(2,1)}, bf16[4,1024,256]{2,1,0:T(8,128)(2,1)}, u32[]{:S(2)}, u32[]{:S(2)}) collective-permute-start(bf16[4,1024,256]{2,1,0:T(8,128)(2,1)} %bitcast.5), channel_id=1, source_target_pairs={{0,1},{1,2},{2,3},{3,0},{4,5},{5,6},{6,7},{7,4},{8,9},{9,10},{10,1... | collective-permute-start | bytes 6291464 | tf_op jit(solution)/shard_map/ppermute | solution.py:28
  63.4 47.6 %collective-permute-start.3 = (bf16[4,1024,256]{2,1,0:T(8,128)(2,1)}, bf16[4,1024,256]{2,1,0:T(8,128)(2,1)}, u32[]{:S(2)}, u32[]{:S(2)}) collective-permute-start(bf16[4,1024,256]{2,1,0:T(8,128)(2,1)} %bitcast.5), channel_id=1, source_target_pairs={{0,3},{1,0},{2,1},{3,2},{4,7},{5,4},{6,5},{7,6},{8,11},{9,8},{10,9... | collective-permute-start | bytes 6291464 | tf_op jit(solution)/shard_map/ppermute | solution.py:30
  96.2 29.0 %collective-permute-start.2 = (bf16[4,1024,256]{2,1,0:T(8,128)(2,1)}, bf16[4,1024,256]{2,1,0:T(8,128)(2,1)}, u32[]{:S(2)}, u32[]{:S(2)}) collective-permute-start(bf16[4,1024,256]{2,1,0:T(8,128)(2,1)} %collective-permute-done.1), channel_id=1, source_target_pairs={{0,1},{1,2},{2,3},{3,0},{4,5},{5,6},{6,7},{7,4},{8,9},{9,10},{10,1... | collective-permute-start | bytes 6291464 | tf_op jit(solution)/shard_map/ppermute | solution.py:28
  101.9 64.3 %collective-permute-start.5 = (bf16[4,1024,256]{2,1,0:T(8,128)(2,1)}, bf16[4,1024,256]{2,1,0:T(8,128)(2,1)}, u32[]{:S(2)}, u32[]{:S(2)}) collective-permute-start(bf16[4,1024,256]{2,1,0:T(8,128)(2,1)} %bitcast.76), channel_id=1, source_target_pairs={{0,1},{1,2},{2,3},{3,0},{4,5},{5,6},{6,7},{7,4},{8,9},{9,10},{10,1... | collective-permute-start | bytes 6291464 | tf_op jit(solution)/shard_map/ppermute | solution.py:28
  103.8 3.6 %copy-start.3 = (bf16[384,1,1024]{2,0,1:T(8,128)(2,1)S(1)}, bf16[384,1,1024]{2,0,1:T(8,128)(2,1)}, u32[]{:S(2)}) copy-start(bf16[384,1,1024]{2,0,1:T(8,128)(2,1)} %fusion.34) | copy-start | bytes 2359300
  103.8 3.6 %copy-start.4 = (bf16[384,1,1024]{2,0,1:T(8,128)(2,1)S(1)}, bf16[384,1,1024]{2,0,1:T(8,128)(2,1)}, u32[]{:S(2)}) copy-start(bf16[384,1,1024]{2,0,1:T(8,128)(2,1)} %get-tuple-element.8) | copy-start | bytes 2359300
  103.8 3.7 %copy-start.5 = (bf16[384,1,1024]{2,0,1:T(8,128)(2,1)S(1)}, bf16[384,1,1024]{2,0,1:T(8,128)(2,1)}, u32[]{:S(2)}) copy-start(bf16[384,1,1024]{2,0,1:T(8,128)(2,1)} %get-tuple-element.9) | copy-start | bytes 2359300
  103.8 3.7 %copy-start.6 = (bf16[384,1,1024]{2,0,1:T(8,128)(2,1)S(1)}, bf16[384,1,1024]{2,0,1:T(8,128)(2,1)}, u32[]{:S(2)}) copy-start(bf16[384,1,1024]{2,0,1:T(8,128)(2,1)} %get-tuple-element.10) | copy-start | bytes 2359300
  155.6 4.6 %copy-start = (f32[384,4096]{1,0:T(8,128)S(1)}, f32[384,4096]{1,0:T(8,128)}, u32[]{:S(2)}) copy-start(f32[384,4096]{1,0:T(8,128)} %reshape_reshape.6) | copy-start | bytes 18874372
  160.2 6.0 %copy-start.9 = (bf16[1,4,1024,256]{3,2,1,0:T(8,128)(2,1)S(1)}, bf16[1,4,1024,256]{3,2,1,0:T(8,128)(2,1)}, u32[]{:S(2)}) copy-start(bf16[1,4,1024,256]{3,2,1,0:T(8,128)(2,1)} %all-gather.7.cloned.1.call-done) | copy-start | bytes 6291460
  161.8 6.3 %collective-permute-start.4 = (bf16[15,4096]{1,0:T(8,128)(2,1)S(1)}, bf16[15,4096]{1,0:T(8,128)(2,1)S(1)}, u32[]{:S(2)}, u32[]{:S(2)}) collective-permute-start(bf16[15,4096]{1,0:T(8,128)(2,1)S(1)} %slice.375), channel_id=1, source_target_pairs={{0,1},{1,2},{2,3},{3,4},{4,5},{5,6},{6,7},{7,8},{8,9},{9,10},{10,1... | collective-permute-start | bytes 368648 | tf_op jit(solution)/shard_map/ppermute | solution.py:44
  166.2 48.5 %collective-permute-start.7 = (bf16[4,1024,256]{2,1,0:T(8,128)(2,1)S(1)}, bf16[4,1024,256]{2,1,0:T(8,128)(2,1)S(1)}, u32[]{:S(2)}, u32[]{:S(2)}) collective-permute-start(bf16[4,1024,256]{2,1,0:T(8,128)(2,1)S(1)} %bitcast.77), channel_id=1, source_target_pairs={{0,3},{1,0},{2,1},{3,2},{4,7},{5,4},{6,5},{7,6},{8,11},{9,8},{10,9... | collective-permute-start | bytes 6291464 | tf_op jit(solution)/shard_map/ppermute | solution.py:30
  166.2 46.9 %collective-permute-start.6 = (bf16[4,1024,256]{2,1,0:T(8,128)(2,1)}, bf16[4,1024,256]{2,1,0:T(8,128)(2,1)S(1)}, u32[]{:S(2)}, u32[]{:S(2)}) collective-permute-start(bf16[4,1024,256]{2,1,0:T(8,128)(2,1)} %collective-permute-done.5), channel_id=1, source_target_pairs={{0,1},{1,2},{2,3},{3,0},{4,5},{5,6},{6,7},{7,4},{8,9},{9,10},{10,1... | collective-permute-start | bytes 6291464 | tf_op jit(solution)/shard_map/ppermute | solution.py:28
Sparse Core Ops, SparseCore 0:
  8.9 44.9 all-gather.4
  55.5 45.9 all-gather.6
